TPU v7x, 32 devices: a whole 2x2x4 slice. The times are simulated.
32 devices in a mesh: rep: 2 (over x), fs: 8 (over z, y), tp: 2 (over core).
Axes of the slice: x: 2, y: 2, z: 4, core: 2. Of those that a mesh axis runs over, the one named last changes fastest.
Arguments:
- tokens: bfloat16 [5120, 2048], P(('rep', 'fs')), may hold values from -6 to 6
- mixer_out: bfloat16 [5120, 2048], P(('rep', 'fs')), may hold values from -6 to 6
- gate_first: bfloat16 [2048, 2816], P('fs', 'tp'), may hold values from -0.125 to 0.125
- up_first: bfloat16 [2048, 2816], P('fs', 'tp'), may hold values from -0.125 to 0.125
- down_first: bfloat16 [2816, 2048], P('tp', 'fs'), may hold values from -0.3125 to 0.3125
- gate_second: bfloat16 [2048, 2816], P('fs', 'tp'), may hold values from -0.125 to 0.125
- up_second: bfloat16 [2048, 2816], P('fs', 'tp'), may hold values from -0.125 to 0.125
- down_second: bfloat16 [2816, 2048], P('tp', 'fs'), may hold values from -0.3125 to 0.3125
- gain_first: float32 [2048], replicated, may hold values from 0.1 to 1.9
- bias_first: float32 [2048], replicated, may hold values from -1.5 to 1.5
- gain_middle: float32 [2048], replicated, may hold values from 0.1 to 1.9
- bias_middle: float32 [2048], replicated, may hold values from -1.5 to 1.5
- gain_last: float32 [2048], replicated, may hold values from 0.1 to 1.9
- bias_last: float32 [2048], replicated, may hold values from -1.5 to 1.5
Outputs:
- layer_out: bfloat16 [5120, 2048], P(('rep', 'fs'))
All inputs are finite; a program needn't handle non-finite values.
Results may differ from a plain program's by a relative error of at most 0.014.
Values may be sent and summed in bfloat16 or wider, within the bound.
A program may use at most 64 MiB of HBM per device.

v0:
```python
import math

import jax
import jax.numpy as jnp
from jax import lax
from jax.sharding import PartitionSpec as P

residual_scale = math.sqrt(2.0)
norm_eps = 1e-05


def normalize(summed, scaling, offset):
    center = summed - jnp.mean(summed, axis=-1, keepdims=True)
    spread = jnp.mean(center * center, axis=-1, keepdims=True)
    return center * lax.rsqrt(spread + norm_eps) * scaling + offset


def add_columns(inputs, portion):
    return jnp.dot(inputs, portion, preferred_element_type=jnp.float32)


def project_in(inputs, gate_weight, up_weight):
    return (
        add_columns(inputs, lax.all_gather(gate_weight, "fs", axis=0, tiled=True)),
        add_columns(inputs, lax.all_gather(up_weight, "fs", axis=0, tiled=True)),
    )


def project_out(hidden, down_weight):
    return jnp.dot(
        hidden,
        lax.all_gather(down_weight, "fs", axis=1, tiled=True),
        preferred_element_type=jnp.float32,
    )


def half_step(inputs, gate_weight, up_weight, down_weight):
    gate, value = project_in(inputs, gate_weight, up_weight)
    hidden = (jax.nn.silu(gate) * value).astype(jnp.bfloat16)
    partials = project_out(hidden, down_weight)
    summed = lax.psum(partials.astype(jnp.bfloat16), "tp")
    return summed


def per_device(
    tokens,
    mixer_out,
    gate_first,
    up_first,
    down_first,
    gate_second,
    up_second,
    down_second,
    gain_first,
    bias_first,
    gain_middle,
    bias_middle,
    gain_last,
    bias_last,
):
    first_branch = half_step(tokens, gate_first, up_first, down_first)
    first_norm = normalize(
        residual_scale * tokens.astype(jnp.float32) + 0.5 * first_branch.astype(jnp.float32),
        gain_first,
        bias_first,
    ).astype(jnp.bfloat16)
    middle_norm = normalize(
        residual_scale * first_norm.astype(jnp.float32) + mixer_out.astype(jnp.float32),
        gain_middle,
        bias_middle,
    ).astype(jnp.bfloat16)
    second_branch = half_step(middle_norm, gate_second, up_second, down_second)
    finished = normalize(
        residual_scale * middle_norm.astype(jnp.float32) + 0.5 * second_branch.astype(jnp.float32),
        gain_last,
        bias_last,
    ).astype(jnp.bfloat16)
    return finished


def solution(mesh):
    return jax.shard_map(
        per_device,
        mesh=mesh,
        in_specs=(
            P(("rep", "fs"), None),
            P(("rep", "fs"), None),
            P("fs", "tp"),
            P("fs", "tp"),
            P("tp", "fs"),
            P("fs", "tp"),
            P("fs", "tp"),
            P("tp", "fs"),
            P(),
            P(),
            P(),
            P(),
            P(),
            P(),
        ),
        out_specs=P(("rep", "fs"), None),
        check_vma=False,
    )
```

profile of v0, /device:TPU:0, one launch (start us, length us, event | category | flops | bytes accessed | tf_op | source)
XLA Modules:
  0.0 639.6 jit_solution(13720102844049315975)
XLA Ops:
  6.5 0.7 all-gather.7.cloned.1.call-update
  7.3 0.0 all-gather.11.cloned.1.call-start
  7.3 0.7 all-gather.11.cloned.1.call-update
  8.0 0.0 all-gather.9.cloned.1.call-start
  8.1 0.7 all-gather.9.cloned.1.call-update
  8.8 0.0 all-reduce.3.cloned.1.call-start
  8.8 95.8 %all-gather.7.cloned.1.call-done = bf16[2048,1408]{1,0:T(8,128)(2,1)} async-done(((bf16[256,1408]{1,0:T(8,128)(2,1)}), bf16[2048,1408]{1,0:T(8,128)(2,1)}) %all-gather.7.cloned.1.call-update) | async-done | bytes 5767184 | tf_op jit(solution)/shard_map/all_gather | solution.py:24
  104.6 5.2 fusion.7
  109.8 88.2 %all-gather.11.cloned.1.call-done = bf16[1408,2048]{1,0:T(8,128)(2,1)} async-done(((bf16[1408,256]{1,0:T(8,128)(2,1)}), bf16[1408,2048]{1,0:T(8,128)(2,1)}) %all-gather.11.cloned.1.call-update) | async-done | bytes 5767184 | tf_op jit(solution)/shard_map/all_gather | solution.py:32
  198.0 92.7 %all-gather.9.cloned.1.call-done = bf16[2048,1408]{1,0:T(8,128)(2,1)} async-done(((bf16[256,1408]{1,0:T(8,128)(2,1)}), bf16[2048,1408]{1,0:T(8,128)(2,1)}) %all-gather.9.cloned.1.call-update) | async-done | bytes 5767184 | tf_op jit(solution)/shard_map/all_gather | solution.py:25
  290.7 9.7 %convolution_convert_fusion.1 = bf16[320,2048]{1,0:T(8,128)(2,1)} fusion(bf16[1408,2048]{1,0:T(8,128)(2,1)} %all-gather.11.cloned.1.call-done, bf16[320,2048]{1,0:T(8,128)(2,1)S(1)} %copy-done.2, bf16[2048,1408]{1,0:T(8,128)(2,1)} %all-gather.9.cloned.1.call-done, f32[320,1408]{1,0:T(8,128)S(1)} %fusion.7), kind=kOutput, calls=%fused_computation.3 | convolution fusion | flops 3694346240 | bytes 15958016 | tf_op jit(solution)/shard_map/dot_general | solution.py:30
  300.4 0.0 all-gather.13.cloned.1.call-start
  300.4 0.5 all-gather.13.cloned.1.call-update
  301.0 0.0 all-gather.15.cloned.1.call-start
  301.0 0.5 all-gather.15.cloned.1.call-update
  301.6 0.7 all-gather.17.cloned.1.call-update
  302.3 0.2 all-reduce.5.cloned.1.call-start
  302.5 16.1 %all-reduce.3.cloned.1.call-done = bf16[320,2048]{1,0:T(8,128)(2,1)} async-done(((bf16[320,2048]{1,0:T(8,128)(2,1)}), bf16[320,2048]{1,0:T(8,128)(2,1)}) %all-reduce.3.cloned.1.call-update) | async-done | bytes 1310736 | tf_op jit(solution)/shard_map/psum | solution.py:41
  318.6 2.0 fusion.3
  320.6 0.8 multiply_reduce_fusion.2
  321.5 1.3 fusion.2
  322.8 0.7 multiply_reduce_fusion.1
  323.5 0.8 add_convert_fusion.1
  324.3 89.9 %all-gather.13.cloned.1.call-done = bf16[2048,1408]{1,0:T(8,128)(2,1)} async-done(((bf16[256,1408]{1,0:T(8,128)(2,1)}), bf16[2048,1408]{1,0:T(8,128)(2,1)}) %all-gather.13.cloned.1.call-update) | async-done | bytes 5767184 | tf_op jit(solution)/shard_map/all_gather | solution.py:24
  414.2 4.8 fusion.8
  419.0 87.7 %all-gather.15.cloned.1.call-done = bf16[2048,1408]{1,0:T(8,128)(2,1)} async-done(((bf16[256,1408]{1,0:T(8,128)(2,1)}), bf16[2048,1408]{1,0:T(8,128)(2,1)}) %all-gather.15.cloned.1.call-update) | async-done | bytes 5767184 | tf_op jit(solution)/shard_map/all_gather | solution.py:25
  506.7 93.4 %all-gather.17.cloned.1.call-done = bf16[1408,2048]{1,0:T(8,128)(2,1)} async-done(((bf16[1408,256]{1,0:T(8,128)(2,1)}), bf16[1408,2048]{1,0:T(8,128)(2,1)}) %all-gather.17.cloned.1.call-update) | async-done | bytes 5767184 | tf_op jit(solution)/shard_map/all_gather | solution.py:32
  600.1 9.7 %convolution_convert_fusion = bf16[320,2048]{1,0:T(8,128)(2,1)} fusion(bf16[1408,2048]{1,0:T(8,128)(2,1)} %all-gather.17.cloned.1.call-done, bf16[320,2048]{1,0:T(8,128)(2,1)S(1)} %add_convert_fusion.1, bf16[2048,1408]{1,0:T(8,128)(2,1)} %all-gather.15.cloned.1.call-done, f32[320,1408]{1,0:T(8,128)S(1)} %fusion.8), kind=kOutput, calls=%fused_computation.2 | convolution fusion | flops 3694346240 | bytes 15958016 | tf_op jit(solution)/shard_map/dot_general | solution.py:30
  609.8 18.2 %all-reduce.5.cloned.1.call-done = bf16[320,2048]{1,0:T(8,128)(2,1)} async-done(((bf16[320,2048]{1,0:T(8,128)(2,1)}), bf16[320,2048]{1,0:T(8,128)(2,1)}) %all-reduce.5.cloned.1.call-update) | async-done | bytes 1310736 | tf_op jit(solution)/shard_map/psum | solution.py:41
  628.0 2.0 fusion.4
  630.0 0.8 multiply_reduce_fusion
  630.9 1.9 add_convert_fusion
  (30 shorter events, 0.2 us)
Async XLA Ops:
  6.5 98.0 %all-gather.7.cloned.1.call-start = ((), (), s32[]{:S(2)}) async-start(), calls=%async_computation | async-start | bytes 6488064 | tf_op jit(solution)/shard_map/all_gather | solution.py:24
  7.3 190.7 %all-gather.11.cloned.1.call-start = ((), (), s32[]{:S(2)}) async-start(), calls=%async_computation.2 | async-start | bytes 6488064 | tf_op jit(solution)/shard_map/all_gather | solution.py:32
  8.0 282.7 %all-gather.9.cloned.1.call-start = ((), (), s32[]{:S(2)}) async-start(), calls=%async_computation.1 | async-start | bytes 6488064 | tf_op jit(solution)/shard_map/all_gather | solution.py:25
  8.7 281.9 %copy-start.2 = (bf16[320,2048]{1,0:T(8,128)(2,1)S(1)}, bf16[320,2048]{1,0:T(8,128)(2,1)}, u32[]{:S(2)}) copy-start(bf16[320,2048]{1,0:T(8,128)(2,1)} %param.14) | copy-start | bytes 3932164
  8.8 309.8 %all-reduce.3.cloned.1.call-start = ((), (), s32[]{:S(2)}) async-start(), calls=%async_computation.3 | async-start | bytes 2621440 | tf_op jit(solution)/shard_map/psum | solution.py:41
  300.4 113.8 %all-gather.13.cloned.1.call-start = ((), (), s32[]{:S(2)}) async-start(), calls=%async_computation.4 | async-start | bytes 6488064 | tf_op jit(solution)/shard_map/all_gather | solution.py:24
  301.0 205.8 %all-gather.15.cloned.1.call-start = ((), (), s32[]{:S(2)}) async-start(), calls=%async_computation.5 | async-start | bytes 6488064 | tf_op jit(solution)/shard_map/all_gather | solution.py:25
  301.5 298.6 %all-gather.17.cloned.1.call-start = ((), (), s32[]{:S(2)}) async-start(), calls=%async_computation.6 | async-start | bytes 6488064 | tf_op jit(solution)/shard_map/all_gather | solution.py:32
  301.6 19.9 %copy-start.4 = (f32[2048]{0:T(1024)S(1)}, f32[2048]{0:T(1024)}, u32[]{:S(2)}) copy-start(f32[2048]{0:T(1024)} %param.23) | copy-start | bytes 24580
  301.6 19.9 %copy-start.5 = (f32[2048]{0:T(1024)S(1)}, f32[2048]{0:T(1024)}, u32[]{:S(2)}) copy-start(f32[2048]{0:T(1024)} %param.22) | copy-start | bytes 24580
  302.3 19.2 %copy-start.1 = (bf16[320,2048]{1,0:T(8,128)(2,1)S(1)}, bf16[320,2048]{1,0:T(8,128)(2,1)}, u32[]{:S(2)}) copy-start(bf16[320,2048]{1,0:T(8,128)(2,1)} %param.15) | copy-start | bytes 3932164
  302.3 325.7 %all-reduce.5.cloned.1.call-start = ((), (), s32[]{:S(2)}) async-start(), calls=%async_computation.7 | async-start | bytes 2621440 | tf_op jit(solution)/shard_map/psum | solution.py:41
  318.6 2.0 copy-start.3
  322.8 0.7 copy-start.6
  322.8 0.7 copy-start.7
  609.8 21.0 %copy-start.8 = (f32[2048]{0:T(1024)S(1)}, f32[2048]{0:T(1024)}, u32[]{:S(2)}) copy-start(f32[2048]{0:T(1024)} %param.27) | copy-start | bytes 24580
  609.8 21.0 %copy-start.9 = (f32[2048]{0:T(1024)S(1)}, f32[2048]{0:T(1024)}, u32[]{:S(2)}) copy-start(f32[2048]{0:T(1024)} %param.26) | copy-start | bytes 24580
  628.0 2.0 copy-start
Sparse Core Ops, SparseCore 0:
  9.5 95.0 all-gather.6
  106.6 91.3 all-gather.10
  200.2 90.4 all-gather.8
  300.5 18.0 all-reduce.2
  320.6 93.4 all-gather.12
  416.2 90.4 all-gather.14
  508.8 91.2 all-gather.16
  609.9 18.0 all-reduce.4
where the time goes:
time: 640 us
  waiting for transfers between devices  586 us (92%)
  matrix products  29.4 us (5%)
  between operations  13.6 us (2%)
  other arithmetic  10.4 us (2%)
    all_gather x2, waiting for transfers between devices, project_in(): lax.all_gather(gate_weight, 'fs', axis=0, tiled=True)  186 us
    all_gather x2, waiting for transfers between devices, project_out(): lax.all_gather(down_weight, 'fs', axis=1, tiled=True)  182 us
    all_gather x2, waiting for transfers between devices, project_in(): lax.all_gather(up_weight, 'fs', axis=0, tiled=True)  180 us
    psum x2, waiting for transfers between devices, half_step(): summed = lax.psum(partials.astype(jnp.bfloat16), 'tp')  34.3 us
    dot_general x2, matrix products, project_out(): jnp.dot(hidden, lax.all_gather(down_weight, 'fs', axis=1, tiled=True), pr...  19.3 us
  transfers between devices with their start and end apart: 8, of which 8 were waited for; matrix products, arithmetic and copies ran while one was open for 2% of the time, Pallas kernels for 0%

commit v1 on v0

v1 whole, which is shorter than its diff:
```python
import functools
import math

import jax
import jax.numpy as jnp
from jax import lax
from jax.experimental import pallas as pl
from jax.experimental.pallas import tpu as pltpu
from jax.sharding import PartitionSpec as P

residual_scale = math.sqrt(2.0)
norm_eps = 1e-05
ZS, YS = 4, 2
F32, BF16 = jnp.float32, jnp.bfloat16


def normalize(summed, scaling, offset):
    center = summed - jnp.mean(summed, axis=-1, keepdims=True)
    spread = jnp.mean(center * center, axis=-1, keepdims=True)
    return center * lax.rsqrt(spread + norm_eps) * scaling + offset


def half_step(inputs, gate_weight, up_weight, down_weight):
    gate = jnp.dot(inputs, lax.all_gather(gate_weight, "fs", axis=0, tiled=True), preferred_element_type=F32)
    value = jnp.dot(inputs, lax.all_gather(up_weight, "fs", axis=0, tiled=True), preferred_element_type=F32)
    hidden = (jax.nn.silu(gate) * value).astype(BF16)
    partials = jnp.dot(hidden, lax.all_gather(down_weight, "fs", axis=1, tiled=True), preferred_element_type=F32)
    return lax.psum(partials.astype(BF16), "tp")


def per_device_general(
    tokens, mixer_out, gate_first, up_first, down_first, gate_second, up_second, down_second,
    gain_first, bias_first, gain_middle, bias_middle, gain_last, bias_last,
):
    first_branch = half_step(tokens, gate_first, up_first, down_first)
    first_norm = normalize(
        residual_scale * tokens.astype(F32) + 0.5 * first_branch.astype(F32), gain_first, bias_first
    ).astype(BF16)
    middle_norm = normalize(
        residual_scale * first_norm.astype(F32) + mixer_out.astype(F32), gain_middle, bias_middle
    ).astype(BF16)
    second_branch = half_step(middle_norm, gate_second, up_second, down_second)
    return normalize(
        residual_scale * middle_norm.astype(F32) + 0.5 * second_branch.astype(F32), gain_last, bias_last
    ).astype(BF16)


def slot(dz, dy):
    return (dz % ZS) * YS + dy % YS


SLOTS = ZS * YS
MESSAGES = {
    "a_p": ((1, 0), (0, 0), "A"),
    "a_m": ((-1, 0), (0, 0), "A"),
    "a_y": ((0, 1), (0, 0), "A"),
    "b_y": ((0, 1), (0, 0), "B"),
    "b_p": ((1, 0), (0, 0), "B"),
    "b_m": ((-1, 0), (0, 0), "B"),
    "a_pf": ((1, 0), (-1, 0), "A1"),
    "a_py": ((0, 1), (-1, 0), "A"),
    "a_mf": ((-1, 0), (1, 0), "A2"),
    "a_my": ((0, 1), (1, 0), "A"),
    "b_yp": ((1, 0), (0, 1), "B"),
    "b_ym": ((-1, 0), (0, 1), "B"),
    "b_mf": ((-1, 0), (1, 0), "B"),
    "a_pfy": ((0, 1), (-2, 0), "A1"),
    "a_mfy": ((0, 1), (2, 0), "A2"),
    "b_ypf": ((1, 0), (-1, 1), "B"),
}
NAMES = list(MESSAGES)


def row_parts(rows):
    a = (rows * 7 // 16) // 16 * 16
    a1 = (a // 2 + 15) // 16 * 16
    return {"A": (0, a), "A1": (0, a1), "A2": (a1, a - a1), "B": (a, rows - a)}


def kernel(
    tokens_ref, mixer_ref, gu1_ref, gu2_ref, d1_ref, d2_ref,
    g1_ref, b1_ref, g2_ref, b2_ref, g3_ref, b3_ref,
    out_ref,
    gu, dn, xb, acc, hid, keep, psend, precv, xsend, xrecv, br, mix, fin,
    wsend, wrecv, xs_send, xs_recv, ds_send, ds_recv, rs_send, rs_recv, local,
):
    rep, fs, core = lax.axis_index("rep"), lax.axis_index("fs"), lax.axis_index("tp")
    z, y = fs // YS, fs % YS
    quarter = fin.shape[0]
    half_hidden = dn.shape[2]
    ks = gu.shape[2]
    dcols = dn.shape[3]

    def fs_of(dz, dy):
        return lax.rem(z + dz + ZS, ZS) * YS + lax.rem(y + dy, YS)

    def plane(dz, dy):
        return {"fs": fs_of(dz, dy)}

    other_rep, other_core = {"rep": 1 - rep}, {"tp": 1 - core}
    mine = pl.ds(pl.multiple_of(core * quarter, quarter), quarter)
    sib = pl.ds(pl.multiple_of((1 - core) * quarter, quarter), quarter)

    hrows = pl.ds(pl.multiple_of(rep * half_hidden, half_hidden), half_hidden)
    own = slot(0, 0)
    loads = [
        pltpu.make_async_copy(gu1_ref, gu.at[0, own], local.at[0]),
        pltpu.make_async_copy(tokens_ref.at[mine], xb.at[0, pl.ds(0, quarter)], local.at[1]),
        pltpu.make_async_copy(tokens_ref.at[sib], xb.at[0, pl.ds(2 * quarter, quarter)], local.at[2]),
        pltpu.make_async_copy(d1_ref.at[hrows], dn.at[0, own], local.at[3]),
        pltpu.make_async_copy(gu2_ref, gu.at[1, own], local.at[4]),
        pltpu.make_async_copy(d2_ref.at[hrows], dn.at[1, own], local.at[5]),
        pltpu.make_async_copy(mixer_ref.at[mine], mix, local.at[6]),
    ]
    for load in loads:
        load.start()

    barrier = pltpu.get_barrier_semaphore()
    for target in (plane(1, 0), plane(-1, 0), plane(0, 1), other_rep, other_core):
        pl.semaphore_signal(barrier, inc=1, device_id=target, device_id_type=pl.DeviceIdType.MESH)
    pl.semaphore_wait(barrier, 5)

    sent = []

    def remote(src, dst, send_sem, recv_sem, target):
        return pltpu.make_async_remote_copy(
            src_ref=src, dst_ref=dst, send_sem=send_sem, recv_sem=recv_sem,
            device_id=target, device_id_type=pl.DeviceIdType.MESH,
        )

    def weight_copy(item, name):
        buf = (gu.at[0], dn.at[0], gu.at[1], dn.at[1])[item]
        (tz, ty), (bz, by), part = MESSAGES[name]
        start, size = row_parts(buf.shape[1])[part]
        rows = pl.ds(start, size)
        at = NAMES.index(name)
        return remote(
            buf.at[slot(bz, by), rows], buf.at[slot(bz - tz, by + ty), rows],
            wsend.at[item, at], wrecv.at[item, at], plane(tz, ty),
        )

    def send(copy):
        copy.start()
        sent.append(copy)

    def start(item, *names):
        for name in names:
            send(weight_copy(item, name))

    def arrived(item, *names):
        for name in names:
            weight_copy(item, name).wait_recv()

    def own_sends(item):
        loads[(0, 3, 4, 5)[item]].wait()
        start(item, "a_p", "a_m", "b_y", "a_y", "b_p", "b_m")

    def share_out(ffn):
        rows = pl.ds(0, quarter)
        send(remote(xb.at[ffn, rows], xb.at[ffn, pl.ds(quarter, quarter)],
                    xs_send.at[ffn], xs_recv.at[ffn], other_rep))

    def share_own(ffn):
        return remote(xb.at[ffn, pl.ds(0, quarter)], xb.at[ffn, pl.ds(2 * quarter, quarter)],
                      ds_send.at[ffn, 0], ds_recv.at[ffn, 0], other_core)

    def share_on(ffn):
        return remote(xb.at[ffn, pl.ds(quarter, quarter)], xb.at[ffn, pl.ds(3 * quarter, quarter)],
                      ds_send.at[ffn, 1], ds_recv.at[ffn, 1], other_core)

    def share_relay(ffn):
        remote(xb.at[ffn, pl.ds(0, quarter)], xb.at[ffn, pl.ds(quarter, quarter)],
               xs_send.at[ffn], xs_recv.at[ffn], other_rep).wait_recv()
        send(share_on(ffn))

    def share_done(ffn):
        if ffn:
            share_own(ffn).wait_recv()
        share_on(ffn).wait_recv()

    rows_step = 2 * quarter

    def gate_up(ffn, *offsets):
        for dz, dy in offsets:
            n = slot(dz, dy)
            cols = pl.ds(pl.multiple_of(fs_of(dz, dy) * ks, ks), ks)

            @pl.loop(0, 2)
            def _(i):
                rows = pl.ds(pl.multiple_of(i * rows_step, rows_step), rows_step)
                part = jnp.dot(xb[ffn, rows, cols], gu[ffn, n], preferred_element_type=F32)
                if n == own:
                    acc[rows, :] = part
                else:
                    acc[rows, :] += part

    def activate():
        low = half_hidden // 128 * 128
        wide = acc.shape[1] - low

        @pl.loop(0, 4 * quarter // 32)
        def _(i):
            rows = pl.ds(pl.multiple_of(i * 32, 32), 32)
            gate = acc[rows, :wide]
            value = acc[rows, low:]
            if half_hidden != low:
                value = pltpu.roll(value, wide - (half_hidden - low), axis=1)
            made = gate / (1.0 + jnp.exp(-gate)) * value
            hid[rows, :] = made[:, :half_hidden].astype(BF16)

    def to_sibling(ffn, n):
        return remote(psend.at[ffn, n], precv.at[ffn, n], rs_send.at[ffn, 0, n], rs_recv.at[ffn, 0, n], other_core)

    def to_pair(ffn, n):
        return remote(xsend.at[ffn, n], xrecv.at[ffn, n], rs_send.at[ffn, 1, n], rs_recv.at[ffn, 1, n], other_rep)

    def down(ffn, *offsets):
        for dz, dy in offsets:
            n = slot(dz, dy)
            whole = jnp.dot(hid[2 * quarter:, :], dn[ffn, n], preferred_element_type=F32)
            psend[ffn, n] = whole.astype(BF16)
            keep[n] = jnp.dot(hid[:2 * quarter, :], dn[ffn, n], preferred_element_type=F32)
            send(to_sibling(ffn, n))
        for dz, dy in offsets:
            n = slot(dz, dy)
            to_sibling(ffn, n).wait_recv()
            xsend[ffn, n] = (keep[n, quarter:, :] + precv[ffn, n, quarter:, :].astype(F32)).astype(BF16)
            keep[n, :quarter, :] = keep[n, :quarter, :] + precv[ffn, n, :quarter, :].astype(F32)
            send(to_pair(ffn, n))

    def collect(ffn, *offsets):
        for dz, dy in offsets:
            n = slot(dz, dy)
            to_pair(ffn, n).wait_recv()
            cols = pl.ds(pl.multiple_of(fs_of(dz, dy) * dcols, dcols), dcols)
            br[:, cols] = keep[n, :quarter, :] + xrecv[ffn, n].astype(F32)

    def first_norms():
        @pl.loop(0, quarter // 16)
        def _(i):
            rows = pl.ds(pl.multiple_of(i * 16, 16), 16)
            first = normalize(
                residual_scale * xb[0, rows, :].astype(F32) + 0.5 * br[rows, :], g1_ref[...], b1_ref[...]
            ).astype(BF16)
            xb[1, rows, :] = normalize(
                residual_scale * first.astype(F32) + mix[rows, :].astype(F32), g2_ref[...], b2_ref[...]
            ).astype(BF16)

    def last_norm():
        @pl.loop(0, quarter // 16)
        def _(i):
            rows = pl.ds(pl.multiple_of(i * 16, 16), 16)
            fin[rows, :] = normalize(
                residual_scale * xb[1, rows, :].astype(F32) + 0.5 * br[rows, :], g3_ref[...], b3_ref[...]
            ).astype(BF16)

    ready_1 = ((0, 1), (1, 0), (-1, 0))
    ready_2 = ((-1, 1), (1, 1))
    ready_3 = ((2, 0), (2, 1))

    for item in range(4):
        ffn = item // 2
        is_gu = item % 2 == 0
        step = functools.partial(gate_up if is_gu else down, ffn)
        if item == 0:
            own_sends(0)
            loads[1].wait()
            share_out(0)
        if item == 1:
            step((0, 0))
        if item == 3:
            step((0, 0))
        arrived(item, "a_p")
        start(item, "a_pf", "a_py")
        arrived(item, "a_m")
        start(item, "a_mf", "a_my")
        arrived(item, "b_y")
        start(item, "b_yp", "b_ym")
        if item == 2:
            collect(0, *ready_3)
            first_norms()
            share_out(1)
            send(share_own(1))
        arrived(item, "b_m")
        start(item, "b_mf")
        arrived(item, "b_p", "a_y")
        if item == 0:
            loads[2].wait()
            share_relay(0)
            share_done(0)
            step((0, 0))
        if item != 2:
            step(*ready_1)
        arrived(item, "a_pf")
        start(item, "a_pfy")
        arrived(item, "a_mf")
        start(item, "a_mfy")
        if item == 2:
            share_relay(1)
            share_done(1)
            step((0, 0), *ready_1)
        arrived(item, "b_yp")
        start(item, "b_ypf")
        arrived(item, "b_ym")
        if item < 3:
            own_sends(item + 1)
        arrived(item, "a_py", "a_my")
        step(*ready_2)
        if not is_gu:
            collect(ffn, (0, 0), *ready_1)
        arrived(item, "b_mf", "a_pfy", "a_mfy", "b_ypf")
        step(*ready_3)
        if is_gu:
            activate()
        else:
            collect(ffn, *ready_2)
            if item == 1:
                loads[6].wait()
    collect(1, *ready_3)
    last_norm()
    put = pltpu.make_async_copy(fin, out_ref.at[mine], local.at[7])
    put.start()
    over = remote(fin, out_ref.at[mine], ds_send.at[0, 0], ds_recv.at[0, 0], other_core)
    over.start()
    over.wait()
    put.wait()
    for copy in sent:
        copy.wait_send()


def per_device(
    tokens, mixer_out, gate_first, up_first, down_first, gate_second, up_second, down_second,
    gain_first, bias_first, gain_middle, bias_middle, gain_last, bias_last,
):
    rows, width = tokens.shape
    ks, hidden = gate_first.shape
    half_hidden = hidden // 2
    dcols = down_first.shape[1]
    quarter = rows // 2
    rep = lax.axis_index("rep")

    def own_half(gate, up):
        at = (0, rep * half_hidden)
        size = (ks, half_hidden)
        return jnp.concatenate([lax.dynamic_slice(gate, at, size), lax.dynamic_slice(up, at, size)], axis=1)

    any_spec, vmem = pl.BlockSpec(memory_space=pl.ANY), pl.BlockSpec(memory_space=pltpu.VMEM)
    vec = lambda v: v.reshape(1, width)
    dma = pltpu.SemaphoreType.DMA
    return pl.pallas_call(
        kernel,
        out_shape=jax.ShapeDtypeStruct((rows, width), BF16),
        in_specs=[any_spec] * 6 + [vmem] * 6,
        out_specs=any_spec,
        scratch_shapes=[
            pltpu.VMEM((2, SLOTS, ks, hidden), BF16),
            pltpu.VMEM((2, SLOTS, half_hidden, dcols), BF16),
            pltpu.VMEM((2, 4 * quarter, width), BF16),
            pltpu.VMEM((4 * quarter, hidden), F32),
            pltpu.VMEM((4 * quarter, half_hidden), BF16),
            pltpu.VMEM((SLOTS, 2 * quarter, dcols), F32),
            pltpu.VMEM((2, SLOTS, 2 * quarter, dcols), BF16),
            pltpu.VMEM((2, SLOTS, 2 * quarter, dcols), BF16),
            pltpu.VMEM((2, SLOTS, quarter, dcols), BF16),
            pltpu.VMEM((2, SLOTS, quarter, dcols), BF16),
            pltpu.VMEM((quarter, width), F32),
            pltpu.VMEM((quarter, width), BF16),
            pltpu.VMEM((quarter, width), BF16),
            dma((4, len(NAMES))), dma((4, len(NAMES))),
            dma((2,)), dma((2,)),
            dma((2, 2)), dma((2, 2)),
            dma((2, 2, SLOTS)), dma((2, 2, SLOTS)),
            dma((8,)),
        ],
        compiler_params=pltpu.CompilerParams(
            collective_id=0, has_side_effects=True, vmem_limit_bytes=60 * 1024 * 1024
        ),
    )(
        tokens, mixer_out, own_half(gate_first, up_first), own_half(gate_second, up_second),
        down_first, down_second,
        vec(gain_first), vec(bias_first), vec(gain_middle), vec(bias_middle), vec(gain_last), vec(bias_last),
    )


def on_mesh(mesh, rows, width, hidden):
    sizes = dict(mesh.shape)
    if (sizes["rep"], sizes["fs"], sizes["tp"]) != (2, SLOTS, 2):
        return False
    rows, ks, hidden = rows // (2 * SLOTS), width // SLOTS, hidden // 2
    return rows % 32 == 0 and ks % 128 == 0 and hidden % 128 == 0 and (hidden // 2) % 64 == 0


def solution(mesh):
    def run(tokens, mixer_out, gate_first, *rest):
        fits = on_mesh(mesh, tokens.shape[0], tokens.shape[1], gate_first.shape[1])
        return jax.shard_map(
            per_device if fits else per_device_general,
            mesh=mesh,
            in_specs=(
                P(("rep", "fs"), None), P(("rep", "fs"), None),
                P("fs", "tp"), P("fs", "tp"), P("tp", "fs"),
                P("fs", "tp"), P("fs", "tp"), P("tp", "fs"),
                P(), P(), P(), P(), P(), P(),
            ),
            out_specs=P(("rep", "fs"), None),
            check_vma=False,
        )(tokens, mixer_out, gate_first, *rest)

    return run
```

time: 640 us -> 246 us (0.38)
  waiting for transfers between devices: 586 us -> 0 us
  Pallas kernels: 0 us -> 239 us
  matrix products: 29.4 us -> 0 us
  between operations: 13.6 us -> 0.03 us
  other arithmetic: 10.4 us -> 2.19 us
    all_gather x6 -> x0, waiting for transfers between devices: 548 us -> none  [the longest x2 186 us: project_in(): lax.all_gather(gate_weight, 'fs', axis=0, tiled=True)]
    pallas_call x0 -> x1, Pallas kernels: none -> 239 us  [per_device(): pl.pallas_call(kernel, out_shape=jax.ShapeDtypeStruct((rows, width), BF16...]
    psum x2 -> x0, waiting for transfers between devices: 34.3 us -> none  [half_step(): summed = lax.psum(partials.astype(jnp.bfloat16), 'tp')]
    dot_general x4 -> x0, matrix products: 29.4 us -> none  [the longest x2 19.3 us: project_out(): jnp.dot(hidden, lax.all_gather(down_weight, 'fs', axis=1, tiled=True), pr...]
    reduce_sum x6 -> x0, other arithmetic: 7.61 us -> none  [the longest x3 5.34 us: normalize(): center = summed - jnp.mean(summed, axis=-1, keepdims=True)]
  transfers between devices with their start and end apart: 8 -> 0, of which waited for: 8 -> 0; matrix products, arithmetic and copies ran while one was open for 2% -> 0% of each run, Pallas kernels for 0% -> 0%
where the time goes in v1:
time: 246 us
  Pallas kernels  239 us (97%)
  local copies, waits for them, and re-layouts  4.68 us (2%)
    pallas_call x1, Pallas kernels, per_device(): pl.pallas_call(kernel, out_shape=jax.ShapeDtypeStruct((rows, width), BF16...  239 us

profile of v1, /device:TPU:0, one launch (start us, length us, event | category | flops | bytes accessed | tf_op | source)
XLA Modules:
  0.0 245.9 jit_solution(17812638433821741984)
XLA Ops:
  0.0 0.0 copy-start
  0.0 0.0 copy-start.1
  0.0 1.7 constant_dynamic-slice_fusion.2
  1.7 1.1 pad_maximum_fusion.gu1_ref
  2.8 0.0 copy-done
  2.8 0.0 copy-done.1
  2.8 0.4 constant_dynamic-slice_fusion
  3.2 1.1 pad_maximum_fusion.1.gu2_ref
  4.4 239.0 %shard_map.136 = bf16[320,2048]{1,0:T(8,128)(2,1)} custom-call(bf16[320,2048]{1,0:T(8,128)(2,1)} %tokens_ref.1, bf16[320,2048]{1,0:T(8,128)(2,1)} %mixer_ref.1, bf16[256,1408]{1,0:T(8,128)(2,1)} %pad_maximum_fusion.gu1_ref, bf16[256,1408]{1,0:T(8,128)(2,1)} %pad_maximum_fusion.1.gu2_ref, bf16[1408,256]{1,0:T(8,128)(2,1)} %d1_ref.1, ...), custom_call_target="tpu_custom_call" | custom-call | tf_op jit(solution)/shard_map/pallas_call | solution.py:350
  243.4 2.5 %copy.16 = bf16[320,2048]{1,0:T(8,128)(2,1)} copy(bf16[320,2048]{1,0:T(8,128)(2,1)} %shard_map.136) | data formatting | bytes 2621440
Async XLA Ops:
  0.0 2.8 %copy-start = (bf16[256,1408]{1,0:T(8,128)(2,1)S(1)}, bf16[256,1408]{1,0:T(8,128)(2,1)}, u32[]{:S(2)}) copy-start(bf16[256,1408]{1,0:T(8,128)(2,1)} %param.20) | copy-start | bytes 2162692
  0.0 2.8 %copy-start.1 = (bf16[256,1408]{1,0:T(8,128)(2,1)S(1)}, bf16[256,1408]{1,0:T(8,128)(2,1)}, u32[]{:S(2)}) copy-start(bf16[256,1408]{1,0:T(8,128)(2,1)} %param.19) | copy-start | bytes 2162692

commit v2 on v1

v2 whole, which is shorter than its diff:
```python
import functools
import math

import jax
import jax.numpy as jnp
from jax import lax
from jax.experimental import pallas as pl
from jax.experimental.pallas import tpu as pltpu
from jax.sharding import PartitionSpec as P

residual_scale = math.sqrt(2.0)
norm_eps = 1e-05
ZS, YS = 4, 2
F32, BF16 = jnp.float32, jnp.bfloat16


def normalize(summed, scaling, offset):
    center = summed - jnp.mean(summed, axis=-1, keepdims=True)
    spread = jnp.mean(center * center, axis=-1, keepdims=True)
    return center * lax.rsqrt(spread + norm_eps) * scaling + offset


def half_step(inputs, gate_weight, up_weight, down_weight):
    gate = jnp.dot(inputs, lax.all_gather(gate_weight, "fs", axis=0, tiled=True), preferred_element_type=F32)
    value = jnp.dot(inputs, lax.all_gather(up_weight, "fs", axis=0, tiled=True), preferred_element_type=F32)
    hidden = (jax.nn.silu(gate) * value).astype(BF16)
    partials = jnp.dot(hidden, lax.all_gather(down_weight, "fs", axis=1, tiled=True), preferred_element_type=F32)
    return lax.psum(partials.astype(BF16), "tp")


def per_device_general(
    tokens, mixer_out, gate_first, up_first, down_first, gate_second, up_second, down_second,
    gain_first, bias_first, gain_middle, bias_middle, gain_last, bias_last,
):
    first_branch = half_step(tokens, gate_first, up_first, down_first)
    first_norm = normalize(
        residual_scale * tokens.astype(F32) + 0.5 * first_branch.astype(F32), gain_first, bias_first
    ).astype(BF16)
    middle_norm = normalize(
        residual_scale * first_norm.astype(F32) + mixer_out.astype(F32), gain_middle, bias_middle
    ).astype(BF16)
    second_branch = half_step(middle_norm, gate_second, up_second, down_second)
    return normalize(
        residual_scale * middle_norm.astype(F32) + 0.5 * second_branch.astype(F32), gain_last, bias_last
    ).astype(BF16)


def slot(dz, dy):
    return (dz % ZS) * YS + dy % YS


SLOTS = ZS * YS
STEPS = range(1, ZS)
NAMES = [("y", 0, 0), ("y", 1, 0)] + [
    (way, d, dy) for way in ("up", "dn", "xup", "xdn") for d in STEPS for dy in range(YS)
]


def kernel(
    tokens_ref, mixer_ref, gu1_ref, gu2_ref, d1_ref, d2_ref,
    g1_ref, b1_ref, g2_ref, b2_ref, g3_ref, b3_ref,
    out_ref,
    gu, dn, xb, acc, hid, keep, psend, precv, xsend, xrecv, br, mix, fin,
    wsend, wrecv, xs_send, xs_recv, ds_send, ds_recv, rs_send, rs_recv, local,
):
    rep, fs, core = lax.axis_index("rep"), lax.axis_index("fs"), lax.axis_index("tp")
    z, y = fs // YS, fs % YS
    quarter = fin.shape[0]
    half_hidden = dn.shape[2]
    ks = gu.shape[2]
    dcols = dn.shape[3]

    def fs_of(dz, dy):
        return lax.rem(z + dz + ZS, ZS) * YS + lax.rem(y + dy, YS)

    def plane(dz, dy):
        return {"fs": fs_of(dz, dy)}

    other_rep, other_core, pair = {"rep": 1 - rep}, {"tp": 1 - core}, plane(0, 1)
    mine = pl.ds(pl.multiple_of(core * quarter, quarter), quarter)
    sib = pl.ds(pl.multiple_of((1 - core) * quarter, quarter), quarter)

    def hrows(who):
        return pl.ds(pl.multiple_of(who * half_hidden, half_hidden), half_hidden)

    own = slot(0, 0)
    loads = [
        pltpu.make_async_copy(gu1_ref.at[y], gu.at[0, own], local.at[0]),
        pltpu.make_async_copy(tokens_ref.at[mine], xb.at[0, pl.ds(0, quarter)], local.at[1]),
        pltpu.make_async_copy(tokens_ref.at[sib], xb.at[0, pl.ds(2 * quarter, quarter)], local.at[2]),
        pltpu.make_async_copy(d1_ref.at[hrows(y)], dn.at[0, own], local.at[3]),
        pltpu.make_async_copy(gu2_ref.at[y], gu.at[1, own], local.at[4]),
        pltpu.make_async_copy(d2_ref.at[hrows(y)], dn.at[1, own], local.at[5]),
        pltpu.make_async_copy(mixer_ref.at[mine], mix, local.at[6]),
    ]
    for load in loads:
        load.start()

    barrier = pltpu.get_barrier_semaphore()

    def greet(target):
        pl.semaphore_signal(barrier, inc=1, device_id=target, device_id_type=pl.DeviceIdType.MESH)

    for target in (pair, other_rep, other_core):
        greet(target)

    @pl.when(z < ZS - 1)
    def _():
        greet(plane(1, 0))

    @pl.when(z > 0)
    def _():
        greet(plane(-1, 0))

    inner = jnp.logical_and(z > 0, z < ZS - 1)

    @pl.when(inner)
    def _():
        pl.semaphore_wait(barrier, 5)

    @pl.when(jnp.logical_not(inner))
    def _():
        pl.semaphore_wait(barrier, 4)

    sent = []

    def remote(src, dst, send_sem, recv_sem, target):
        return pltpu.make_async_remote_copy(
            src_ref=src, dst_ref=dst, send_sem=send_sem, recv_sem=recv_sem,
            device_id=target, device_id_type=pl.DeviceIdType.MESH,
        )

    def send(copy):
        copy.start()
        sent.append(copy)

    weights = (gu.at[0], dn.at[0], gu.at[1], dn.at[1])

    def weight_copy(item, name):
        way, d, dy = name
        buf = weights[item]
        rows = buf.shape[1] // 2
        part = pl.ds(pl.multiple_of(rep * rows, rows), rows)
        sems = wsend.at[item, NAMES.index(name)], wrecv.at[item, NAMES.index(name)]
        if way == "y":
            at = rep if d == 0 else 1 - rep
            part = pl.ds(pl.multiple_of(at * rows, rows), rows)
            if item % 2 == 0:
                src = (gu1_ref, None, gu2_ref)[item].at[1 - y, part]
            else:
                first = (1 - y) * half_hidden + at * rows
                src = (None, d1_ref, None, d2_ref)[item].at[pl.ds(pl.multiple_of(first, rows), rows)]
            return remote(src, buf.at[slot(0, 1), part], *sems, pair)
        sign = -1 if way in ("up", "xup") else 1
        there = buf.at[slot(sign * d, dy), part]
        if way in ("xup", "xdn"):
            return remote(there, there, *sems, other_rep)
        return remote(buf.at[slot(sign * (d - 1), dy), part], there, *sems, plane(-sign, 0))

    def sends_up(d):
        return jnp.logical_and(z >= d - 1, z < ZS - 1)

    def sends_dn(d):
        return jnp.logical_and(z + d - 1 <= ZS - 1, z > 0)

    def gets_up(d):
        return z >= d

    def gets_dn(d):
        return z + d <= ZS - 1

    def line_start(item, d, dy):
        @pl.when(sends_up(d))
        def _():
            weight_copy(item, ("up", d, dy)).start()

        @pl.when(sends_dn(d))
        def _():
            weight_copy(item, ("dn", d, dy)).start()

    def relay(item, d, dy):
        for way, gets in (("up", gets_up), ("dn", gets_dn)):
            @pl.when(gets(d))
            def _():
                weight_copy(item, (way, d, dy)).wait_recv()
                if d < ZS - 1:
                    @pl.when((sends_up if way == "up" else sends_dn)(d + 1))
                    def _():
                        weight_copy(item, (way, d + 1, dy)).start()
                weight_copy(item, ("x" + way, d, dy)).start()

    def swapped(item, d):
        for way, gets in (("xup", gets_up), ("xdn", gets_dn)):
            @pl.when(gets(d))
            def _():
                for dy in range(YS):
                    weight_copy(item, (way, d, dy)).wait_recv()

    def pair_start(item, part):
        send(weight_copy(item, ("y", part, 0)))

    def pair_wait(item, part):
        weight_copy(item, ("y", part, 0)).wait_recv()

    def share_out(ffn):
        return remote(xb.at[ffn, pl.ds(0, quarter)], xb.at[ffn, pl.ds(quarter, quarter)],
                      xs_send.at[ffn], xs_recv.at[ffn], pair)

    def share_own(ffn):
        return remote(xb.at[ffn, pl.ds(0, quarter)], xb.at[ffn, pl.ds(2 * quarter, quarter)],
                      ds_send.at[ffn, 0], ds_recv.at[ffn, 0], other_core)

    def share_on(ffn):
        return remote(xb.at[ffn, pl.ds(quarter, quarter)], xb.at[ffn, pl.ds(3 * quarter, quarter)],
                      ds_send.at[ffn, 1], ds_recv.at[ffn, 1], other_core)

    def share_finish(ffn):
        share_out(ffn).wait_recv()
        send(share_on(ffn))
        if ffn:
            share_own(ffn).wait_recv()
        share_on(ffn).wait_recv()

    rows_step = 2 * quarter

    def gate_up_slot(ffn, dz, dy, first=False):
        n = slot(dz, 0) + dy
        cols = pl.ds(pl.multiple_of(fs_of(dz, dy) * ks, ks), ks)

        @pl.loop(0, 2)
        def _(i):
            rows = pl.ds(pl.multiple_of(i * rows_step, rows_step), rows_step)
            part = jnp.dot(xb[ffn, rows, cols], gu[ffn, n], preferred_element_type=F32)
            if first:
                acc[rows, :] = part
            else:
                acc[rows, :] += part

    def at_distance(d, act):
        for dz, gets in ((-d, gets_up), (d, gets_dn)):
            @pl.when(gets(d))
            def _():
                @pl.loop(0, YS)
                def _(dy):
                    act(dz, dy)

    def activate():
        low = half_hidden // 128 * 128
        wide = acc.shape[1] - low

        @pl.loop(0, 4 * quarter // 32)
        def _(i):
            rows = pl.ds(pl.multiple_of(i * 32, 32), 32)
            gate = acc[rows, :wide]
            value = acc[rows, low:]
            if half_hidden != low:
                value = pltpu.roll(value, wide - (half_hidden - low), axis=1)
            made = gate / (1.0 + jnp.exp(-gate)) * value
            hid[rows, :] = made[:, :half_hidden].astype(BF16)

    def to_sibling(ffn, n):
        return remote(psend.at[ffn, n], precv.at[ffn, n], rs_send.at[ffn, 0, n], rs_recv.at[ffn, 0, n], other_core)

    def to_pair(ffn, dz, dy):
        n, there = slot(dz, 0) + dy, slot(dz, 0) + 1 - dy
        return remote(xsend.at[ffn, n], xrecv.at[ffn, there], rs_send.at[ffn, 1, n], rs_recv.at[ffn, 1, there], pair)

    def from_pair(ffn, n):
        return remote(xsend.at[ffn, n], xrecv.at[ffn, n], rs_send.at[ffn, 1, n], rs_recv.at[ffn, 1, n], pair)

    def down_slot(ffn, dz, dy):
        n = slot(dz, 0) + dy
        whole = jnp.dot(hid[2 * quarter:, :], dn[ffn, n], preferred_element_type=F32)
        psend[ffn, n] = whole.astype(BF16)
        keep[n] = jnp.dot(hid[:2 * quarter, :], dn[ffn, n], preferred_element_type=F32)
        to_sibling(ffn, n).start()

    def add_cores(ffn, dz, dy):
        n = slot(dz, 0) + dy
        to_sibling(ffn, n).wait_recv()
        xsend[ffn, n] = (keep[n, quarter:, :] + precv[ffn, n, quarter:, :].astype(F32)).astype(BF16)
        keep[n, :quarter, :] = keep[n, :quarter, :] + precv[ffn, n, :quarter, :].astype(F32)
        to_pair(ffn, dz, dy).start()

    def collect_slot(ffn, dz, dy):
        n = slot(dz, 0) + dy
        from_pair(ffn, n).wait_recv()
        cols = pl.ds(pl.multiple_of(fs_of(dz, dy) * dcols, dcols), dcols)
        br[:, cols] = keep[n, :quarter, :] + xrecv[ffn, n].astype(F32)

    def first_norms():
        @pl.loop(0, quarter // 16)
        def _(i):
            rows = pl.ds(pl.multiple_of(i * 16, 16), 16)
            first = normalize(
                residual_scale * xb[0, rows, :].astype(F32) + 0.5 * br[rows, :], g1_ref[...], b1_ref[...]
            ).astype(BF16)
            xb[1, rows, :] = normalize(
                residual_scale * first.astype(F32) + mix[rows, :].astype(F32), g2_ref[...], b2_ref[...]
            ).astype(BF16)

    def last_norm():
        @pl.loop(0, quarter // 16)
        def _(i):
            rows = pl.ds(pl.multiple_of(i * 16, 16), 16)
            fin[rows, :] = normalize(
                residual_scale * xb[1, rows, :].astype(F32) + 0.5 * br[rows, :], g3_ref[...], b3_ref[...]
            ).astype(BF16)

    def open_item(item):
        pair_start(item, 0)
        loads[(0, 3, 4, 5)[item]].wait()
        line_start(item, 1, 0)

    def second_start(item):
        pair_wait(item, 0)
        line_start(item, 1, 1)

    def work(item, d):
        ffn = item // 2
        if item % 2 == 0:
            at_distance(d, lambda dz, dy: gate_up_slot(ffn, dz, dy))
        else:
            at_distance(d, lambda dz, dy: down_slot(ffn, dz, dy))
            at_distance(d, lambda dz, dy: add_cores(ffn, dz, dy))

    def work_near(item, dy):
        ffn = item // 2
        if item % 2 == 0:
            gate_up_slot(ffn, 0, dy, first=dy == 0)
        else:
            down_slot(ffn, 0, dy)
            add_cores(ffn, 0, dy)

    def finish(item):
        ffn = item // 2
        for d in range(2, ZS):
            swapped(item, d)
            work(item, d)
        if item % 2 == 0:
            activate()
        else:
            for dy in range(YS):
                collect_slot(ffn, 0, dy)
            for d in STEPS:
                at_distance(d, lambda dz, dy: collect_slot(ffn, dz, dy))

    for item in range(4):
        if item == 0:
            open_item(0)
            loads[1].wait()
            send(share_out(0))
            pair_start(0, 1)
            second_start(0)
        relay(item, 1, 0)
        if item:
            finish(item - 1)
        if item == 2:
            loads[6].wait()
            first_norms()
            send(share_out(1))
            send(share_own(1))
            pair_start(2, 1)
        relay(item, 1, 1)
        if item == 0:
            loads[2].wait()
            share_finish(0)
        if item != 2:
            work_near(item, 0)
            pair_wait(item, 1)
            work_near(item, 1)
        for dy in range(YS):
            relay(item, 2, dy)
        if item < 3:
            open_item(item + 1)
            if item + 1 != 2:
                pair_start(item + 1, 1)
        if item == 2:
            share_finish(1)
            work_near(2, 0)
            pair_wait(2, 1)
            work_near(2, 1)
        relay(item, 3, 0)
        if item < 3:
            second_start(item + 1)
        swapped(item, 1)
        work(item, 1)
        relay(item, 3, 1)
    finish(3)
    last_norm()
    put = pltpu.make_async_copy(fin, out_ref.at[mine], local.at[7])
    put.start()
    over = remote(fin, out_ref.at[mine], ds_send.at[0, 0], ds_recv.at[0, 0], other_core)
    over.start()
    over.wait()
    put.wait()
    for copy in sent:
        copy.wait_send()
    for ffn in range(2):
        for n in range(SLOTS):
            to_sibling(ffn, n).wait_send()
            from_pair(ffn, n).wait_send()
    for item in range(4):
        for d in STEPS:
            for way, does in (("up", sends_up), ("dn", sends_dn), ("xup", gets_up), ("xdn", gets_dn)):
                @pl.when(does(d))
                def _():
                    for dy in range(YS):
                        weight_copy(item, (way, d, dy)).wait_send()


def per_device(
    tokens, mixer_out, gate_first, up_first, down_first, gate_second, up_second, down_second,
    gain_first, bias_first, gain_middle, bias_middle, gain_last, bias_last,
):
    rows, width = tokens.shape
    ks, hidden = gate_first.shape
    half_hidden = hidden // 2
    dcols = down_first.shape[1]
    quarter = rows // 2

    def halves(gate, up):
        return jnp.stack(
            [
                jnp.concatenate([w[:, at:at + half_hidden] for w in (gate, up)], axis=1)
                for at in (0, half_hidden)
            ]
        )

    any_spec, vmem = pl.BlockSpec(memory_space=pl.ANY), pl.BlockSpec(memory_space=pltpu.VMEM)
    vec = lambda v: v.reshape(1, width)
    dma = pltpu.SemaphoreType.DMA
    return pl.pallas_call(
        kernel,
        out_shape=jax.ShapeDtypeStruct((rows, width), BF16),
        in_specs=[any_spec] * 6 + [vmem] * 6,
        out_specs=any_spec,
        scratch_shapes=[
            pltpu.VMEM((2, SLOTS, ks, hidden), BF16),
            pltpu.VMEM((2, SLOTS, half_hidden, dcols), BF16),
            pltpu.VMEM((2, 4 * quarter, width), BF16),
            pltpu.VMEM((4 * quarter, hidden), F32),
            pltpu.VMEM((4 * quarter, half_hidden), BF16),
            pltpu.VMEM((SLOTS, 2 * quarter, dcols), F32),
            pltpu.VMEM((2, SLOTS, 2 * quarter, dcols), BF16),
            pltpu.VMEM((2, SLOTS, 2 * quarter, dcols), BF16),
            pltpu.VMEM((2, SLOTS, quarter, dcols), BF16),
            pltpu.VMEM((2, SLOTS, quarter, dcols), BF16),
            pltpu.VMEM((quarter, width), F32),
            pltpu.VMEM((quarter, width), BF16),
            pltpu.VMEM((quarter, width), BF16),
            dma((4, len(NAMES))), dma((4, len(NAMES))),
            dma((2,)), dma((2,)),
            dma((2, 2)), dma((2, 2)),
            dma((2, 2, SLOTS)), dma((2, 2, SLOTS)),
            dma((8,)),
        ],
        compiler_params=pltpu.CompilerParams(
            collective_id=0, has_side_effects=True, vmem_limit_bytes=60 * 1024 * 1024
        ),
    )(
        tokens, mixer_out, halves(gate_first, up_first), halves(gate_second, up_second),
        down_first, down_second,
        vec(gain_first), vec(bias_first), vec(gain_middle), vec(bias_middle), vec(gain_last), vec(bias_last),
    )


def on_mesh(mesh, rows, width, hidden):
    sizes = dict(mesh.shape)
    if (sizes["rep"], sizes["fs"], sizes["tp"]) != (2, SLOTS, 2):
        return False
    rows, ks, hidden = rows // (2 * SLOTS), width // SLOTS, hidden // 2
    return rows % 32 == 0 and ks % 128 == 0 and hidden % 128 == 0 and (hidden // 2) % 64 == 0


def solution(mesh):
    def run(tokens, mixer_out, gate_first, *rest):
        fits = on_mesh(mesh, tokens.shape[0], tokens.shape[1], gate_first.shape[1])
        return jax.shard_map(
            per_device if fits else per_device_general,
            mesh=mesh,
            in_specs=(
                P(("rep", "fs"), None), P(("rep", "fs"), None),
                P("fs", "tp"), P("fs", "tp"), P("tp", "fs"),
                P("fs", "tp"), P("fs", "tp"), P("tp", "fs"),
                P(), P(), P(), P(), P(), P(),
            ),
            out_specs=P(("rep", "fs"), None),
            check_vma=False,
        )(tokens, mixer_out, gate_first, *rest)

    return run
```

time: 246 us -> 194 us (0.79)
  Pallas kernels: 239 us -> 185 us
    pallas_call x1, Pallas kernels: 239 us -> 185 us  [per_device(): pl.pallas_call(kernel, out_shape=jax.ShapeDtypeStruct((rows, width), BF16...]
    another operation x0 -> x4, other arithmetic: none -> 3.38 us  [halves(): jnp.stack([jnp.concatenate([w[:, at:at + half_hidden] for w in (gate, up)...]
where the time goes in v2:
time: 194 us
  Pallas kernels  185 us (95%)
  local copies, waits for them, and re-layouts  5.33 us (3%)
  other arithmetic  3.38 us (2%)
    pallas_call x1, Pallas kernels, per_device(): pl.pallas_call(kernel, out_shape=jax.ShapeDtypeStruct((rows, width), BF16...  185 us

profile of v2, /device:TPU:0, one launch (start us, length us, event | category | flops | bytes accessed | tf_op | source)
XLA Modules:
  0.0 193.6 jit_solution(3283093862302236219)
XLA Ops:
  0.0 0.0 copy-start
  0.0 1.4 fusion.2
  1.4 0.0 copy-done
  1.4 0.2 fusion.3
  1.6 0.4 maximum_bitcast_fusion
  2.0 0.0 copy-start.1
  2.0 1.3 pad_maximum_fusion.gu1_ref
  3.3 0.0 copy-done.1
  3.3 0.0 copy-start.2
  3.3 0.2 fusion
  3.4 0.9 copy-done.2
  4.4 0.2 fusion.1
  4.6 0.4 maximum_bitcast_fusion.2
  5.0 1.3 pad_maximum_fusion.1.gu2_ref
  6.2 184.9 %shard_map.136 = bf16[320,2048]{1,0:T(8,128)(2,1)} custom-call(bf16[320,2048]{1,0:T(8,128)(2,1)} %tokens_ref.1, bf16[320,2048]{1,0:T(8,128)(2,1)} %mixer_ref.1, bf16[2,256,1408]{2,1,0:T(8,128)(2,1)} %pad_maximum_fusion.gu1_ref, bf16[2,256,1408]{2,1,0:T(8,128)(2,1)} %pad_maximum_fusion.1.gu2_ref, bf16[1408,256]{1,0:T(8,128)(2,1)} %d1_ref.1, ...), custom_call_target="tpu_custom_call" | custom-call | tf_op jit(solution)/shard_map/pallas_call | solution.py:433
  191.1 2.5 %copy.16 = bf16[320,2048]{1,0:T(8,128)(2,1)} copy(bf16[320,2048]{1,0:T(8,128)(2,1)} %shard_map.136) | data formatting | bytes 2621440
Async XLA Ops:
  0.0 1.4 copy-start
  2.0 1.3 copy-start.1
  3.3 1.1 copy-start.2
